TPU v7x, 32 devices: a whole 2x2x4 slice. The times are simulated.
32 devices in a mesh: fs: 4 (over z), rep: 4 (over y, x), tp: 2 (over core).
Axes of the slice: x: 2, y: 2, z: 4, core: 2. Of those that a mesh axis runs over, the one named last changes fastest.
Arguments:
- saved_input: bfloat16 [16384, 2048], P(('fs', 'rep')), may hold values from -6 to 6
- value_cotangent: bfloat16 [16384, 4096], P(('fs', 'rep'), 'tp'), may hold values from -0.0061950684 to 0.0061950684
- factor: bfloat16 [2048, 128], P('fs'), may hold values from -1.5 to 1.5
- weight: float32 [2048, 4096], P('fs', 'tp'), may hold values from -1.2 to 1.2
- first_moment: float32 [128, 4096], P('fs', 'tp'), may hold values from -1.8 to 1.8
- second_moment: float32 [128, 4096], P('fs', 'tp'), may hold values from 0.1 to 1
Outputs:
- low_grad: float32 [128, 4096], P('fs', 'tp')
- new_first: float32 [128, 4096], P('fs', 'tp')
- new_second: float32 [128, 4096], P('fs', 'tp')
- direction: float32 [2048, 4096], P('fs', 'tp')
- new_weight: float32 [2048, 4096], P('fs', 'tp')
- new_copy: bfloat16 [2048, 4096], P('fs', 'tp')
All inputs are finite; a program needn't handle non-finite values.
Results may differ from a plain program's by a relative error of at most 0.006.
Values may be sent and summed in bfloat16 or wider, within the bound.
A program may use at most 64 MiB of HBM per device.

v0:
```python
import jax
import jax.numpy as jnp
from jax import lax
from jax.sharding import PartitionSpec as P

D = 2048
E = 4096
first_decay = 0.9
second_decay = 0.9
learn_rate = 0.05
epsilon = 1e-08


def on_device(saved_input, value_cotangent, factor, weight, first_moment, second_moment):
    factor_wide = factor.astype(jnp.float32)
    factor_whole = lax.all_gather(factor, "fs", axis=0, tiled=True)
    projected = jnp.dot(saved_input, factor_whole, preferred_element_type=jnp.float32)
    upper = projected.astype(jnp.bfloat16)
    lower = (projected - upper.astype(jnp.float32)).astype(jnp.bfloat16)
    dims = (((0,), (0,)), ((), ()))
    high_part = lax.dot_general(upper, value_cotangent, dims, preferred_element_type=jnp.float32)
    low_part = lax.dot_general(lower, value_cotangent, dims, preferred_element_type=jnp.float32)
    low_grad = lax.psum_scatter(high_part + low_part, "fs", scatter_dimension=0, tiled=True)
    low_grad = lax.psum(low_grad, "rep")
    new_first = first_decay * first_moment + (1.0 - first_decay) * low_grad
    new_second = second_decay * second_moment + (1.0 - second_decay) * low_grad * low_grad
    ratio = new_first / (jnp.sqrt(new_second) + epsilon)
    ratio_whole = lax.all_gather(ratio, "fs", axis=0, tiled=True)
    raw = jnp.dot(factor_wide, ratio_whole, precision=lax.Precision.HIGHEST)
    total = lax.psum(jnp.sum(raw * raw), ("fs", "tp"))
    spread = jnp.sqrt(total / (D * E))
    direction = raw / (spread + 1.0)
    new_weight = weight - learn_rate * direction
    return (low_grad, new_first, new_second, direction, new_weight, new_weight.astype(jnp.bfloat16))


def solution(mesh):
    placed = (
        P(("fs", "rep"), None),
        P(("fs", "rep"), "tp"),
        P("fs", None),
        P("fs", "tp"),
        P("fs", "tp"),
        P("fs", "tp"),
    )
    return jax.shard_map(
        on_device,
        mesh=mesh,
        in_specs=placed,
        out_specs=(
            P("fs", "tp"),
            P("fs", "tp"),
            P("fs", "tp"),
            P("fs", "tp"),
            P("fs", "tp"),
            P("fs", "tp"),
        ),
        check_vma=False,
    )
```

profile of v0, /device:TPU:0, one launch (start us, length us, event | category | flops | bytes accessed | tf_op | source)
XLA Modules:
  0.0 185.3 jit_solution(11213346444921834174)
XLA Ops:
  7.2 0.0 reduce-scatter.2.cloned.1.call-start
  7.2 17.7 %all_gather.6 = bf16[2048,128]{1,0:T(8,128)(2,1)S(1)} all-gather(bf16[512,128]{1,0:T(8,128)(2,1)} %param.8), channel_id=1, replica_groups=mesh['fs'=4,'rep'=4,'tp'=2] {'fs'}, dimensions={0}, use_global_device_ids=true | all-gather | bytes 655360 | tf_op jit(solution)/shard_map/all_gather | solution.py:16
  24.9 3.4 %fusion.6 = f32[1024,128]{1,0:T(8,128)S(1)} fusion(bf16[1024,2048]{1,0:T(8,128)(2,1)} %param.6, bf16[2048,128]{1,0:T(8,128)(2,1)S(1)} %all_gather.6), kind=kOutput, calls=%fused_computation.13 | convolution fusion | flops 536870912 | bytes 5242880 | tf_op jit(solution)/shard_map/dot_general | solution.py:17
  28.4 0.7 fusion.2
  29.1 0.0 copy-start.3
  29.2 1.7 convolution_add_fusion
  30.9 0.0 reduce-scatter.2.cloned.1.call-update
  30.9 0.0 all-reduce.2.cloned.1.call-start
  31.0 29.2 %reduce-scatter.2.cloned.1.call-done = f32[32,2048]{1,0:T(8,128)} async-done(((f32[128,2048]{1,0:T(8,128)}), f32[32,2048]{1,0:T(8,128)}) %reduce-scatter.2.cloned.1.call-update) | async-done | bytes 262160 | tf_op jit(solution)/shard_map/reduce_scatter | solution.py:23
  60.1 0.0 all-reduce.2.cloned.1.call-update
  60.1 0.0 all-gather.2.cloned.1.call-start
  60.2 44.5 %all-reduce.2.cloned.1.call-done = f32[32,2048]{1,0:T(8,128)} async-done(((f32[32,2048]{1,0:T(8,128)}), f32[32,2048]{1,0:T(8,128)}) %all-reduce.2.cloned.1.call-update) | async-done | bytes 262160 | tf_op jit(solution)/shard_map/psum | solution.py:24
  104.6 1.9 %add_divide_fusion = (f32[32,2048]{1,0:T(8,128)}, f32[32,2048]{1,0:T(8,128)}, f32[32,2048]{1,0:T(8,128)}) fusion(f32[32,2048]{1,0:T(8,128)} %all-reduce.2.cloned.1.call-done, f32[32,2048]{1,0:T(8,128)S(1)} %copy-done.3, f32[32,2048]{1,0:T(8,128)S(1)} %copy-done.4), kind=kLoop, calls=%fused_computation.8 | loop fusion | flops 524288 | bytes 1572864 | tf_op jit(solution)/shard_map/div | solution.py:27
  106.5 0.0 all-gather.2.cloned.1.call-update
  106.6 0.0 copy-start.2
  106.6 5.4 %copy.12 = f32[512,2048]{0,1:T(8,128)} copy(f32[512,2048]{1,0:T(8,128)} %param.9) | data formatting | bytes 8388608 | tf_op args[3]
  112.0 22.8 %all-gather.2.cloned.1.call-done = f32[128,2048]{1,0:T(8,128)} async-done(((f32[32,2048]{1,0:T(8,128)}), f32[128,2048]{1,0:T(8,128)}) %all-gather.2.cloned.1.call-update) | async-done | bytes 1048592 | tf_op jit(solution)/shard_map/all_gather | solution.py:28
  134.8 6.0 %multiply_reduce_fusion = (f32[]{:T(128)}, f32[2048,512]{1,0:T(8,128)}) fusion(f32[128,2048]{1,0:T(8,128)} %all-gather.2.cloned.1.call-done, bf16[512,128]{1,0:T(8,128)(2,1)S(1)} %copy-done.2), kind=kOutput, calls=%fused_computation.2 | convolution fusion | flops 1612709888 | bytes 5373956 | tf_op jit(solution)/shard_map/dot_general | solution.py:29
  140.8 15.3 %psum.15 = f32[]{:T(128)} all-reduce(f32[]{:T(128)} %get-tuple-element.18), channel_id=1, replica_groups=mesh['fs'=4,'rep'=4,'tp'=2] {'fs','tp'}, use_global_device_ids=true, to_apply=%region_3.0 | all-reduce | flops 1 | bytes 8 | tf_op jit(solution)/shard_map/psum | solution.py:30
  156.7 8.3 %fusion.4 = (bf16[512,2048]{0,1:T(8,128)(2,1)S(1)}, f32[512,2048]{0,1:T(8,128)}, f32[512,2048]{0,1:T(8,128)}) fusion(f32[512,2048]{0,1:T(8,128)} %copy.12, f32[2048,512]{1,0:T(8,128)} %get-tuple-element.19, f32[]{:T(128)S(6)} %add.29), kind=kLoop, calls=%fused_computation.12 | loop fusion | flops 4194304 | bytes 18874372 | tf_op jit(solution)/shard_map/convert_element_type | solution.py:34
  165.0 2.4 %copy.15 = bf16[512,2048]{1,0:T(8,128)(2,1)} copy(bf16[512,2048]{0,1:T(8,128)(2,1)S(1)} %get-tuple-element.12) | data formatting | bytes 4194304
  167.4 5.3 %copy.14 = f32[512,2048]{1,0:T(8,128)} copy(f32[512,2048]{0,1:T(8,128)} %get-tuple-element.13) | data formatting | bytes 8388608
  172.7 5.4 %copy.13 = f32[512,2048]{1,0:T(8,128)} copy(f32[512,2048]{0,1:T(8,128)} %get-tuple-element.14) | data formatting | bytes 8388608
  178.1 0.7 copy.17
  (8 shorter events, 0.0 us)
Async XLA Ops:
  7.2 52.9 %reduce-scatter.2.cloned.1.call-start = ((), (), s32[]{:S(2)}) async-start(), calls=%async_computation.1 | async-start | bytes 1310720 | tf_op jit(solution)/shard_map/reduce_scatter | solution.py:23
  7.2 21.2 %copy-start = (bf16[1024,2048]{1,0:T(8,128)(2,1)S(1)}, bf16[1024,2048]{1,0:T(8,128)(2,1)}, u32[]{:S(2)}) copy-start(bf16[1024,2048]{1,0:T(8,128)(2,1)} %param.7) | copy-start | bytes 12582916
  29.1 75.5 %copy-start.3 = (f32[32,2048]{1,0:T(8,128)S(1)}, f32[32,2048]{1,0:T(8,128)}, u32[]{:S(2)}) copy-start(f32[32,2048]{1,0:T(8,128)} %param.11) | copy-start | bytes 786436
  29.1 75.5 %copy-start.4 = (f32[32,2048]{1,0:T(8,128)S(1)}, f32[32,2048]{1,0:T(8,128)}, u32[]{:S(2)}) copy-start(f32[32,2048]{1,0:T(8,128)} %param.10) | copy-start | bytes 786436
  30.9 73.7 %all-reduce.2.cloned.1.call-start = ((), (), s32[]{:S(2)}) async-start(), calls=%async_computation.2 | async-start | bytes 524288 | tf_op jit(solution)/shard_map/psum | solution.py:24
  60.1 74.7 %all-gather.2.cloned.1.call-start = ((), (), s32[]{:S(2)}) async-start(), calls=%async_computation.3 | async-start | bytes 1310720 | tf_op jit(solution)/shard_map/all_gather | solution.py:28
  106.6 28.2 %copy-start.2 = (bf16[512,128]{1,0:T(8,128)(2,1)S(1)}, bf16[512,128]{1,0:T(8,128)(2,1)}, u32[]{:S(2)}) copy-start(bf16[512,128]{1,0:T(8,128)(2,1)} %param.8) | copy-start | bytes 393220
  172.7 5.4 %copy-start.1 = (f32[32,2048]{1,0:T(8,128)S(1)}, f32[32,2048]{1,0:T(8,128)}, u32[]{:S(2)}) copy-start(f32[32,2048]{1,0:T(8,128)} %all-reduce.2.cloned.1.call-done) | copy-start | bytes 786436
Sparse Core Ops, SparseCore 0:
  31.0 29.0 reduce-scatter.1
  63.0 41.5 all-reduce.1
  106.8 27.9 all-gather.1
where the time goes:
time: 186 us; the launch traced here: 185 us
  waiting for transfers between devices  96.5 us (52%)
  blocking collectives  33 us (18%)
  local copies, waits for them, and re-layouts  19.2 us (10%)
  between operations  14.5 us (8%)
  matrix products  11.9 us (6%)
  other arithmetic  10.2 us (5%)
    psum x1, waiting for transfers between devices, on_device(): low_grad = lax.psum(low_grad, 'rep')  44.5 us
    reduce_scatter x1, waiting for transfers between devices, on_device(): lax.psum_scatter(high_part + low_part, 'fs', scatter_dimension=0, tiled=T...  29.2 us
    all_gather x1, waiting for transfers between devices, on_device(): ratio_whole = lax.all_gather(ratio, 'fs', axis=0, tiled=True)  22.8 us
    unnamed x15, local copies, waits for them, and re-layouts  19.2 us
    all_gather x1, blocking collectives, on_device(): factor_whole = lax.all_gather(factor, 'fs', axis=0, tiled=True)  17.7 us
    psum x1, blocking collectives, on_device(): total = lax.psum(jnp.sum(raw * raw), ('fs', 'tp'))  15.3 us
    convert_element_type x1, other arithmetic, on_device(): new_weight.astype(jnp.bfloat16)  8.28 us
    dot_general x1, matrix products, on_device(): raw = jnp.dot(factor_wide, ratio_whole, precision=lax.Precision.HIGHEST)  5.95 us
  transfers between devices with their start and end apart: 3, of which 3 were waited for; matrix products, arithmetic and copies ran while one was open for 3% of the time, Pallas kernels for 0%

commit v1 on v0

--- a/solution.py
+++ b/solution.py
@@ -25,7 +25,14 @@
     new_first = first_decay * first_moment + (1.0 - first_decay) * low_grad
     new_second = second_decay * second_moment + (1.0 - second_decay) * low_grad * low_grad
     ratio = new_first / (jnp.sqrt(new_second) + epsilon)
-    ratio_whole = lax.all_gather(ratio, "fs", axis=0, tiled=True)
+    devices = lax.axis_size("fs")
+    right = [(i, (i + 1) % devices) for i in range(devices)]
+    parts = [ratio]
+    for far in range(1, devices):
+        parts = [lax.ppermute(parts[0], "fs", right), *parts]
+    full = jnp.concatenate(parts, axis=0)
+    turn = (lax.axis_index("fs") + 1) * parts[-1].shape[0]
+    ratio_whole = jnp.roll(full, turn, axis=0)
     raw = jnp.dot(factor_wide, ratio_whole, precision=lax.Precision.HIGHEST)
     total = lax.psum(jnp.sum(raw * raw), ("fs", "tp"))
     spread = jnp.sqrt(total / (D * E))

time: 186 us -> 182 us (0.978)
  waiting for transfers between devices: 96.5 us -> 92.9 us
    all_gather x1 -> x0, waiting for transfers between devices: 22.8 us -> none  [on_device(): ratio_whole = lax.all_gather(ratio, 'fs', axis=0, tiled=True)]
    ppermute x0 -> x3, waiting for transfers between devices: none -> 19.2 us  [on_device(): parts = [lax.ppermute(parts[0], 'fs', right), *parts]]
    unnamed x15 -> x22, local copies, waits for them, and re-layouts: 19.2 us -> 19.3 us
  transfers between devices with their start and end apart: 3 -> 5, of which waited for: 3 -> 5; matrix products, arithmetic and copies ran while one was open for 3% -> 3% of each run, Pallas kernels for 0% -> 0%
where the time goes in v1:
time: 182 us; the launch traced here: 181 us
  waiting for transfers between devices  92.9 us (51%)
  blocking collectives  31.8 us (17%)
  local copies, waits for them, and re-layouts  19.3 us (11%)
  between operations  14.8 us (8%)
  matrix products  10.8 us (6%)
  other arithmetic  10.2 us (6%)
    psum x1, waiting for transfers between devices, on_device(): low_grad = lax.psum(low_grad, 'rep')  44.5 us
    reduce_scatter x1, waiting for transfers between devices, on_device(): lax.psum_scatter(high_part + low_part, 'fs', scatter_dimension=0, tiled=T...  29.2 us
    unnamed x22, local copies, waits for them, and re-layouts  19.3 us
    ppermute x3, waiting for transfers between devices, on_device(): parts = [lax.ppermute(parts[0], 'fs', right), *parts]  19.2 us
    all_gather x1, blocking collectives, on_device(): factor_whole = lax.all_gather(factor, 'fs', axis=0, tiled=True)  17.6 us
    psum x1, blocking collectives, on_device(): total = lax.psum(jnp.sum(raw * raw), ('fs', 'tp'))  14.2 us
    convert_element_type x1, other arithmetic, on_device(): new_weight.astype(jnp.bfloat16)  8.28 us
    dot_general x1, matrix products, on_device(): raw = jnp.dot(factor_wide, ratio_whole, precision=lax.Precision.HIGHEST)  4.79 us
  transfers between devices with their start and end apart: 5, of which 5 were waited for; matrix products, arithmetic and copies ran while one was open for 3% of the time, Pallas kernels for 0%

profile of v1, /device:TPU:0, one launch (start us, length us, event | category | flops | bytes accessed | tf_op | source)
XLA Modules:
  0.0 181.4 jit_solution(15899201904070606418)
XLA Ops:
  7.2 0.0 reduce-scatter.2.cloned.1.call-start
  7.2 17.6 %all_gather.3 = bf16[2048,128]{1,0:T(8,128)(2,1)S(1)} all-gather(bf16[512,128]{1,0:T(8,128)(2,1)} %param.8), channel_id=1, replica_groups=mesh['fs'=4,'rep'=4,'tp'=2] {'fs'}, dimensions={0}, use_global_device_ids=true | all-gather | bytes 655360 | tf_op jit(solution)/shard_map/all_gather | solution.py:16
  24.8 3.6 %fusion.9 = f32[1024,128]{1,0:T(8,128)S(1)} fusion(bf16[1024,2048]{1,0:T(8,128)(2,1)} %param.6, bf16[2048,128]{1,0:T(8,128)(2,1)S(1)} %all_gather.3), kind=kOutput, calls=%fused_computation.24 | convolution fusion | flops 536870912 | bytes 5242880 | tf_op jit(solution)/shard_map/dot_general | solution.py:17
  28.4 0.7 fusion.4
  29.1 0.0 copy-start.3
  29.2 1.7 convolution_add_fusion
  30.9 0.0 reduce-scatter.2.cloned.1.call-update
  30.9 0.0 all-reduce.2.cloned.1.call-start
  31.0 29.2 %reduce-scatter.2.cloned.1.call-done = f32[32,2048]{1,0:T(8,128)} async-done(((f32[128,2048]{1,0:T(8,128)}), f32[32,2048]{1,0:T(8,128)}) %reduce-scatter.2.cloned.1.call-update) | async-done | bytes 262160 | tf_op jit(solution)/shard_map/reduce_scatter | solution.py:23
  60.1 0.0 all-reduce.2.cloned.1.call-update
  60.1 44.5 %all-reduce.2.cloned.1.call-done = f32[32,2048]{1,0:T(8,128)} async-done(((f32[32,2048]{1,0:T(8,128)}), f32[32,2048]{1,0:T(8,128)}) %all-reduce.2.cloned.1.call-update) | async-done | bytes 262160 | tf_op jit(solution)/shard_map/psum | solution.py:24
  104.6 1.9 %add_divide_fusion = (f32[32,2048]{1,0:T(8,128)S(1)}, f32[32,2048]{1,0:T(8,128)}, f32[32,2048]{1,0:T(8,128)}) fusion(f32[32,2048]{1,0:T(8,128)} %all-reduce.2.cloned.1.call-done, f32[32,2048]{1,0:T(8,128)S(1)} %copy-done.3, f32[32,2048]{1,0:T(8,128)S(1)} %copy-done.4), kind=kLoop, calls=%fused_computation.10 | loop fusion | flops 524288 | bytes 1572864 | tf_op jit(solution)/shard_map/div | solution.py:27
  106.5 1.5 collective-permute-start
  108.0 7.9 %collective-permute-done = f32[32,2048]{1,0:T(8,128)S(1)} collective-permute-done((f32[32,2048]{1,0:T(8,128)S(1)}, f32[32,2048]{1,0:T(8,128)S(1)}, u32[]{:S(2)}, u32[]{:S(2)}) %collective-permute-start) | collective-permute-done | bytes 262176 | tf_op jit(solution)/shard_map/ppermute | solution.py:32
  115.9 8.5 %collective-permute-done.1 = f32[32,2048]{1,0:T(8,128)S(1)} collective-permute-done((f32[32,2048]{1,0:T(8,128)S(1)}, f32[32,2048]{1,0:T(8,128)S(1)}, u32[]{:S(2)}, u32[]{:S(2)}) %collective-permute-start.1) | collective-permute-done | bytes 262176 | tf_op jit(solution)/shard_map/ppermute | solution.py:32
  124.4 5.3 %copy.12 = f32[512,2048]{0,1:T(8,128)} copy(f32[512,2048]{1,0:T(8,128)} %param.9) | data formatting | bytes 8388608 | tf_op args[3]
  129.7 2.8 %collective-permute-done.2 = f32[32,2048]{1,0:T(8,128)S(1)} collective-permute-done((f32[32,2048]{1,0:T(8,128)S(1)}, f32[32,2048]{1,0:T(8,128)S(1)}, u32[]{:S(2)}, u32[]{:S(2)}) %collective-permute-start.2) | collective-permute-done | bytes 262176 | tf_op jit(solution)/shard_map/ppermute | solution.py:32
  132.8 4.8 %multiply_reduce_fusion = (f32[]{:T(128)}, f32[2048,512]{1,0:T(8,128)}) fusion(bf16[512,128]{1,0:T(8,128)(2,1)S(1)} %copy-done.2, f32[256,2048]{1,0:T(8,128)S(1)} %constant_dynamic-update-slice_fusion, s32[]{:T(128)S(6)} %select_n.14), kind=kOutput, calls=%fused_computation.2 | convolution fusion | flops 1612709888 | bytes 5373960 | tf_op jit(solution)/shard_map/dot_general | solution.py:36
  137.6 14.2 %psum.15 = f32[]{:T(128)} all-reduce(f32[]{:T(128)} %get-tuple-element.18), channel_id=1, replica_groups=mesh['fs'=4,'rep'=4,'tp'=2] {'fs','tp'}, use_global_device_ids=true, to_apply=%region_3.4 | all-reduce | flops 1 | bytes 8 | tf_op jit(solution)/shard_map/psum | solution.py:37
  152.5 8.3 %fusion.7 = (bf16[512,2048]{0,1:T(8,128)(2,1)S(1)}, f32[512,2048]{0,1:T(8,128)}, f32[512,2048]{0,1:T(8,128)}) fusion(f32[512,2048]{0,1:T(8,128)} %copy.12, f32[2048,512]{1,0:T(8,128)} %get-tuple-element.19, f32[]{:T(128)S(6)} %add.45), kind=kLoop, calls=%fused_computation.23 | loop fusion | flops 4194304 | bytes 18874372 | tf_op jit(solution)/shard_map/convert_element_type | solution.py:41
  160.8 2.4 %copy.15 = bf16[512,2048]{1,0:T(8,128)(2,1)} copy(bf16[512,2048]{0,1:T(8,128)(2,1)S(1)} %get-tuple-element.12) | data formatting | bytes 4194304
  163.1 5.3 %copy.14 = f32[512,2048]{1,0:T(8,128)} copy(f32[512,2048]{0,1:T(8,128)} %get-tuple-element.13) | data formatting | bytes 8388608
  168.5 5.4 %copy.13 = f32[512,2048]{1,0:T(8,128)} copy(f32[512,2048]{0,1:T(8,128)} %get-tuple-element.14) | data formatting | bytes 8388608
  173.9 0.7 copy.24
  (19 shorter events, 0.2 us)
Async XLA Ops:
  7.2 53.0 %reduce-scatter.2.cloned.1.call-start = ((), (), s32[]{:S(2)}) async-start(), calls=%async_computation.1 | async-start | bytes 1310720 | tf_op jit(solution)/shard_map/reduce_scatter | solution.py:23
  24.8 3.6 %copy-start = (bf16[1024,2048]{1,0:T(8,128)(2,1)S(1)}, bf16[1024,2048]{1,0:T(8,128)(2,1)}, u32[]{:S(2)}) copy-start(bf16[1024,2048]{1,0:T(8,128)(2,1)} %param.7) | copy-start | bytes 12582916
  29.1 75.5 %copy-start.3 = (f32[32,2048]{1,0:T(8,128)S(1)}, f32[32,2048]{1,0:T(8,128)}, u32[]{:S(2)}) copy-start(f32[32,2048]{1,0:T(8,128)} %param.11) | copy-start | bytes 786436
  29.2 75.5 %copy-start.4 = (f32[32,2048]{1,0:T(8,128)S(1)}, f32[32,2048]{1,0:T(8,128)}, u32[]{:S(2)}) copy-start(f32[32,2048]{1,0:T(8,128)} %param.10) | copy-start | bytes 786436
  30.9 73.7 %all-reduce.2.cloned.1.call-start = ((), (), s32[]{:S(2)}) async-start(), calls=%async_computation.2 | async-start | bytes 524288 | tf_op jit(solution)/shard_map/psum | solution.py:24
  106.5 9.4 %collective-permute-start = (f32[32,2048]{1,0:T(8,128)S(1)}, f32[32,2048]{1,0:T(8,128)S(1)}, u32[]{:S(2)}, u32[]{:S(2)}) collective-permute-start(f32[32,2048]{1,0:T(8,128)S(1)} %get-tuple-element.15), channel_id=1, source_target_pairs={{0,8},{8,16},{16,24},{24,0},{1,9},{9,17},{17,25},{25,1},{2,10},{10... | collective-permute-start | bytes 786440 | tf_op jit(solution)/shard_map/ppermute | solution.py:32
  115.9 8.5 %collective-permute-start.1 = (f32[32,2048]{1,0:T(8,128)S(1)}, f32[32,2048]{1,0:T(8,128)S(1)}, u32[]{:S(2)}, u32[]{:S(2)}) collective-permute-start(f32[32,2048]{1,0:T(8,128)S(1)} %collective-permute-done), channel_id=1, source_target_pairs={{0,8},{8,16},{16,24},{24,0},{1,9},{9,17},{17,25},{25,1},{2,10},{10... | collective-permute-start | bytes 786440 | tf_op jit(solution)/shard_map/ppermute | solution.py:32
  124.4 8.2 %collective-permute-start.2 = (f32[32,2048]{1,0:T(8,128)S(1)}, f32[32,2048]{1,0:T(8,128)S(1)}, u32[]{:S(2)}, u32[]{:S(2)}) collective-permute-start(f32[32,2048]{1,0:T(8,128)S(1)} %collective-permute-done.1), channel_id=1, source_target_pairs={{0,8},{8,16},{16,24},{24,0},{1,9},{9,17},{17,25},{25,1},{2,10},{10... | collective-permute-start | bytes 786440 | tf_op jit(solution)/shard_map/ppermute | solution.py:32
  129.7 3.0 %copy-start.2 = (bf16[512,128]{1,0:T(8,128)(2,1)S(1)}, bf16[512,128]{1,0:T(8,128)(2,1)}, u32[]{:S(2)}) copy-start(bf16[512,128]{1,0:T(8,128)(2,1)} %param.8) | copy-start | bytes 393220
  168.5 5.4 %copy-start.1 = (f32[32,2048]{1,0:T(8,128)S(1)}, f32[32,2048]{1,0:T(8,128)}, u32[]{:S(2)}) copy-start(f32[32,2048]{1,0:T(8,128)} %all-reduce.2.cloned.1.call-done) | copy-start | bytes 786436
Sparse Core Ops, SparseCore 0:
  31.0 29.0 reduce-scatter.1
  63.0 41.5 all-reduce.1
